TPU v7x, 32 devices: a whole 2x2x4 slice. The times are simulated.
32 devices in a mesh: grp: 1, ep: 32 (over z, y, x, core).
Axes of the slice: x: 2, y: 2, z: 4, core: 2. Of those that a mesh axis runs over, the one named last changes fastest.
Arguments:
- residual_input: bfloat16 [768, 2048], P(('grp', 'ep')), may hold values from -6 to 6
- attention_norm_gain: bfloat16 [2048], replicated, may hold values from 0.099609375 to 1.8984375
- receptance_weight: bfloat16 [2048, 1024], P(None, 'ep'), may hold values from -0.125 to 0.125
- key_weight: bfloat16 [2048, 1024], P(None, 'ep'), may hold values from -0.125 to 0.125
- value_weight: bfloat16 [2048, 1024], P(None, 'ep'), may hold values from -0.125 to 0.125
- decay_weight: bfloat16 [2048, 1024], P(None, 'ep'), may hold values from -0.125 to 0.125
- correction_rate_weight: bfloat16 [2048, 1024], P(None, 'ep'), may hold values from -0.125 to 0.125
- output_gate_weight: bfloat16 [2048, 1024], P(None, 'ep'), may hold values from -0.125 to 0.125
- decay_offset: float32 [1024], replicated, may hold values from -3 to 1
- correction_rate_offset: float32 [1024], replicated, may hold values from -1.5 to 1.5
- self_term_weight: float32 [1024], replicated, may hold values from -2 to 2
- head_read_gain: float32 [1024], replicated, may hold values from 0.1 to 1.9
- previous_state: float32 [768, 16, 4096], P(('grp', 'ep')), may hold values from -4 to 4
- attention_output_weight: bfloat16 [1024, 2048], replicated, may hold values from -0.1875 to 0.1875
- feedforward_norm_gain: bfloat16 [2048], replicated, may hold values from 0.099609375 to 1.8984375
- routes: int32 [768, 4], P('grp'), may hold values from 0 to 31, all different within a row; in each aligned block of 24 rows (0 to 23, 24 to 47, ...) at most 4 rows name the same one
- routing_weight: float32 [768, 4], P('grp'), may hold values from 0.2 to 1
- routed_gate_weight: bfloat16 [32, 2048, 512], P('ep'), may hold values from -0.125 to 0.125
- routed_up_weight: bfloat16 [32, 2048, 512], P('ep'), may hold values from -0.125 to 0.125
- routed_down_weight: bfloat16 [32, 512, 2048], P('ep'), may hold values from -0.25 to 0.25
- common_gate_weight: bfloat16 [2048, 512], replicated, may hold values from -0.125 to 0.125
- common_up_weight: bfloat16 [2048, 512], replicated, may hold values from -0.125 to 0.125
- common_down_weight: bfloat16 [512, 2048], replicated, may hold values from -0.25 to 0.25
Outputs:
- hidden_out: bfloat16 [768, 2048], P(('grp', 'ep'))
- next_state: float32 [768, 16, 4096], P(('grp', 'ep'))
Inputs may be any that keep to these rules, and one draw needn't show every extreme that they name: `routes`: the 4 entries of a row differ. In each aligned block of 24 rows (the tokens of one index of ep) no expert is named by more than 4 rows, a bound that some block reaches.
All inputs are finite; a program needn't handle non-finite values.
Results may differ from a plain program's by a relative error of at most 0.013.
Values may be sent and summed in bfloat16 or wider, within the bound.
A program may use at most 128 MiB of HBM per device.

v0:
```python
import jax
import jax.numpy as jnp
from jax import lax
from jax.sharding import PartitionSpec as P

HEAD_COUNT = 16
HEAD_SIZE = 64
CAP = 4


def rms_norm(value_rows, gain):
    scale = lax.rsqrt(jnp.mean(value_rows * value_rows, axis=-1, keepdims=True) + 1e-06)
    return (value_rows * scale * gain.astype(jnp.float32)).astype(jnp.bfloat16)


def expert_mlp(rows, gate_w, up_w, down_w):
    gate = jnp.dot(rows, gate_w, preferred_element_type=jnp.float32)
    upward = jnp.dot(rows, up_w, preferred_element_type=jnp.float32)
    hidden = (jax.nn.silu(gate) * upward).astype(jnp.bfloat16)
    return jnp.dot(hidden, down_w, preferred_element_type=jnp.float32).astype(jnp.bfloat16)


def attention_mixer(
    receptance_rows,
    key_rows,
    value_rows,
    decay_logit,
    rate_logit,
    gate_logit,
    decay_offset,
    correction_rate_offset,
    self_term_weight,
    head_read_gain,
    head_state,
):
    tally_value = receptance_rows.shape[0]

    def heads(tensor):
        return tensor.astype(jnp.float32).reshape(tally_value, HEAD_COUNT, HEAD_SIZE)

    decay = jnp.exp(
        -jnp.exp(-jax.nn.softplus(-(decay_offset + decay_logit.astype(jnp.float32))) - 0.5)
    )
    rate = jax.nn.sigmoid(correction_rate_offset + rate_logit.astype(jnp.float32))
    key_head = heads(key_rows)
    rate_head = heads(rate)
    receptance_head = heads(receptance_rows)
    head_value = heads(value_rows)
    unit_key = key_head * lax.rsqrt(1.0 + jnp.sum(key_head * key_head, axis=-1, keepdims=True))
    rate_scaled_key = key_head * rate_head
    removal = unit_key * rate_head
    matrix = head_state.reshape(tally_value, HEAD_COUNT, HEAD_SIZE, HEAD_SIZE)
    recalled = jnp.einsum("nhvk,nhk->nhv", matrix, unit_key, precision=lax.Precision.HIGHEST)
    matrix = (
        matrix * heads(decay)[:, :, None, :]
        - recalled[..., None] * removal[:, :, None, :]
        + head_value[..., None] * rate_scaled_key[:, :, None, :]
    )
    read = jnp.einsum("nhvk,nhk->nhv", matrix, receptance_head, precision=lax.Precision.HIGHEST)
    centered = read - jnp.mean(read, axis=-1, keepdims=True)
    variance = jnp.mean(centered * centered, axis=-1, keepdims=True)
    normed_head_read = (
        centered * lax.rsqrt(variance + 0.00064) * head_read_gain.reshape(HEAD_COUNT, HEAD_SIZE)
    )
    self_term = (
        jnp.sum(
            receptance_head * rate_scaled_key * self_term_weight.reshape(HEAD_COUNT, HEAD_SIZE),
            axis=-1,
            keepdims=True,
        )
        * head_value
    )
    normed_mixer_input = (normed_head_read + self_term).reshape(
        tally_value, HEAD_COUNT * HEAD_SIZE
    ) * jax.nn.sigmoid(gate_logit.astype(jnp.float32))
    return (
        normed_mixer_input.astype(jnp.bfloat16),
        matrix.reshape(tally_value, HEAD_COUNT, HEAD_SIZE * HEAD_SIZE),
    )


def slot_table(block_routes, block_weight, expert_ids):
    match = block_routes[..., None] == expert_ids
    hit = jnp.any(match, axis=-2).astype(jnp.int32)
    weight = jnp.sum(jnp.where(match, block_weight[..., None], 0.0), axis=-2)
    rank = jnp.cumsum(hit, axis=-2) - hit
    slots = jnp.arange(CAP, dtype=jnp.int32)
    select = ((hit[..., None] == 1) & (rank[..., None] == slots)).astype(jnp.float32)
    return (select, weight)


def combine_returned(select, weight, returned):
    coefficient = select * weight[..., None]
    return jnp.einsum(
        "nec,ecd->nd", coefficient, returned.astype(jnp.float32), precision=lax.Precision.HIGHEST
    )


def serve_gathered(
    whole, routes, routing_weight, ep_size, tally_value, expert_ids, gate_w, up_w, down_w
):
    block_routes = routes.reshape(ep_size, tally_value, routes.shape[-1])
    block_weight = routing_weight.reshape(ep_size, tally_value, routing_weight.shape[-1])
    select, weight = slot_table(block_routes, block_weight, expert_ids)
    select = select[:, :, 0, :]
    weight = weight[:, :, 0]
    rows = jnp.einsum(
        "snc,snd->scd",
        select.astype(jnp.bfloat16),
        whole.reshape(ep_size, tally_value, whole.shape[-1]),
        preferred_element_type=jnp.float32,
    ).astype(jnp.bfloat16)
    output = expert_mlp(rows.reshape(-1, rows.shape[-1]), gate_w, up_w, down_w).reshape(rows.shape)
    return (output, select, weight)


def per_device(
    residual_input,
    attention_norm_gain,
    receptance_weight,
    key_weight,
    value_weight,
    decay_weight,
    correction_rate_weight,
    output_gate_weight,
    decay_offset,
    correction_rate_offset,
    self_term_weight,
    head_read_gain,
    previous_state,
    attention_output_weight,
    feedforward_norm_gain,
    routes,
    routing_weight,
    routed_gate_weight,
    routed_up_weight,
    routed_down_weight,
    common_gate_weight,
    common_up_weight,
    common_down_weight,
):
    ep_size = lax.axis_size("ep")
    device = lax.axis_index("ep")
    tally_value = residual_input.shape[0]
    normed = rms_norm(residual_input.astype(jnp.float32), attention_norm_gain)
    stacked = jnp.stack(
        (
            receptance_weight,
            key_weight,
            value_weight,
            decay_weight,
            correction_rate_weight,
            output_gate_weight,
        ),
        axis=1,
    )
    local_cols = jnp.einsum(
        "td,drc->trc",
        lax.all_gather(normed, "ep", axis=0, tiled=True),
        stacked,
        preferred_element_type=jnp.float32,
    ).astype(jnp.bfloat16)
    role_rows = lax.all_to_all(local_cols, "ep", split_axis=0, concat_axis=2, tiled=True)
    normed_mixer_input, next_state = attention_mixer(
        role_rows[:, 0],
        role_rows[:, 1],
        role_rows[:, 2],
        role_rows[:, 3],
        role_rows[:, 4],
        role_rows[:, 5],
        decay_offset,
        correction_rate_offset,
        self_term_weight,
        head_read_gain,
        previous_state,
    )
    attended = jnp.dot(
        normed_mixer_input, attention_output_weight, preferred_element_type=jnp.float32
    ).astype(jnp.bfloat16)
    middle = residual_input.astype(jnp.float32) + attended.astype(jnp.float32)
    normed_ffn = rms_norm(middle, feedforward_norm_gain)
    shared = expert_mlp(normed_ffn, common_gate_weight, common_up_weight, common_down_weight)
    expert_count = routed_gate_weight.shape[0] * ep_size
    all_ids = jnp.arange(expert_count, dtype=jnp.int32)
    own_ids = device.reshape(1)
    own_routes = lax.dynamic_slice_in_dim(routes, device * tally_value, tally_value, 0)
    own_weight = lax.dynamic_slice_in_dim(routing_weight, device * tally_value, tally_value, 0)
    whole = lax.all_gather(normed_ffn, "ep", axis=0, tiled=True)
    output, unused_select, unused_weight = serve_gathered(
        whole,
        routes,
        routing_weight,
        ep_size,
        tally_value,
        own_ids,
        routed_gate_weight[0],
        routed_up_weight[0],
        routed_down_weight[0],
    )
    returned = lax.all_to_all(output, "ep", split_axis=0, concat_axis=0, tiled=True)
    select, weight = slot_table(own_routes, own_weight, all_ids)
    routed = combine_returned(select, weight, returned)
    hidden_out = (middle + shared.astype(jnp.float32) + routed).astype(jnp.bfloat16)
    return (hidden_out, next_state)


def solution(mesh):
    return jax.shard_map(
        per_device,
        mesh=mesh,
        in_specs=(
            P(("grp", "ep"), None),
            P(),
            P(None, "ep"),
            P(None, "ep"),
            P(None, "ep"),
            P(None, "ep"),
            P(None, "ep"),
            P(None, "ep"),
            P(),
            P(),
            P(),
            P(),
            P(("grp", "ep"), None, None),
            P(),
            P(),
            P("grp", None),
            P("grp", None),
            P("ep", None, None),
            P("ep", None, None),
            P("ep", None, None),
            P(),
            P(),
            P(),
        ),
        out_specs=(P(("grp", "ep"), None), P(("grp", "ep"), None, None)),
        check_vma=False,
    )
```

profile of v0, /device:TPU:0, one launch (start us, length us, event | category | flops | bytes accessed | tf_op | source)
XLA Modules:
  0.0 249.9 jit_solution(6900193728107449112)
XLA Ops:
  7.2 0.8 convert_element_type.171
  8.1 1.0 fusion.34
  9.1 1.6 fusion.36
  10.7 0.9 bitcast_dynamic-update-slice_fusion.5
  11.7 0.9 bitcast_dynamic-update-slice_fusion.4
  12.6 0.9 bitcast_dynamic-update-slice_fusion.3
  13.5 0.9 bitcast_dynamic-update-slice_fusion.2
  14.4 0.9 bitcast_dynamic-update-slice_fusion.1
  15.3 0.9 bitcast_dynamic-update-slice_fusion
  16.3 57.0 %all-gather.3.cloned.1.call-done = bf16[768,2048]{1,0:T(8,128)(2,1)} async-done(((bf16[24,2048]{1,0:T(8,128)(2,1)}), bf16[768,2048]{1,0:T(8,128)(2,1)}) %all-gather.3.cloned.1.call-update) | async-done | bytes 3145744 | tf_op jit(solution)/shard_map/all_gather | solution.py:159
  73.2 3.1 %fusion.72 = f32[768,192]{0,1:S(1)} fusion(bf16[768,2048]{1,0:T(8,128)(2,1)} %all-gather.3.cloned.1.call-done, bf16[2048,192]{0,1:T(8,128)(2,1)S(1)} %bitcast.99), kind=kOutput, calls=%fused_computation.110 | convolution fusion | flops 603979776 | bytes 4521984
  76.4 1.8 copy.38
  78.2 3.4 %reshape.259 = bf16[32,2,2304]{2,1,0:T(2,128)(2,1)} reshape(bf16[768,6,32]{2,1,0:T(8,128)(2,1)} %copy.38) | data formatting | bytes 589824
  81.6 3.3 %all-to-all-start = ((bf16[32,2,2304]{2,1,0:T(2,128)(2,1)}), bf16[32,2,2304]{2,1,0:T(2,128)(2,1)S(1)}, u32[]{:S(2)}, u32[]{:S(2)}) async-start(bf16[32,2,2304]{2,1,0:T(2,128)(2,1)} %reshape.259), calls=%async_computation | async-start | bytes 589824 | tf_op jit(solution)/shard_map/all_to_all | solution.py:163
  85.0 0.2 all-gather.5.cloned.1.call-start
  85.3 10.8 %reshape.237 = f32[24,16,64,64]{3,2,1,0:T(8,128)} reshape(f32[24,16,4096]{2,1,0:T(8,128)} %param.35) | data formatting | bytes 12582912 | tf_op jit(solution)/shard_map/reshape | solution.py:52
  96.4 2.2 reshape.260
  98.6 2.2 copy.40
  100.8 1.9 all_to_all.19
  102.7 0.9 slice_convert_fusion.2
  103.6 0.8 reshape.258
  105.1 0.2 fusion.41
  105.5 22.8 %fusion.73 = f32[24,16,1,64]{3,2,1,0:T(1,128)S(1)} fusion(f32[24,16,64,1]{2,3,1,0:T(1,128)S(1)} %bitcast.97, f32[24,16,64,64]{3,2,1,0:T(8,128)} %reshape.237), kind=kOutput, calls=%fused_computation.111 | convolution fusion | flops 18874368 | bytes 6488064 | tf_op jit(solution)/shard_map/nhvk,nhk->nhv/dot_general | solution.py:53
  128.3 16.5 %fusion.1 = f32[24,16,1,64]{3,2,1,0:T(1,128)S(1)} fusion(bf16[24,16,64,1]{2,3,1,0:T(2,128)(2,1)S(1)} %copy-done.6, f32[24,16,64,64]{3,2,1,0:T(8,128)S(1)} %copy-done.1, f32[24,16,64]{2,1,0:T(8,128)S(1)} %fusion.41, f32[24,16,64]{2,1,0:T(8,128)S(1)} %get-tuple-element.2, f32[24,16,64]{2,1,0:T(8,128)S(1)} %bitcast.95, f32[24,16,64]{2,1,0:T(8,128)S(1)} %get-tuple-element.4, ...), kind=kOutput, calls=%fused_computation.1 | convolution fusion | flops 26738688 | bytes 6930432 | tf_op jit(solution)/shard_map/nhvk,nhk->nhv/dot_general | solution.py:59
  144.9 0.2 multiply_reduce_fusion.1
  145.2 0.8 fusion.24
  146.1 3.0 %multiply_reduce_fusion = (f32[24]{0:T(128)S(1)}, f32[24,2048]{1,0:T(8,128)S(1)}) fusion(bf16[1024,2048]{1,0:T(8,128)(2,1)} %param.36, f32[24,1024]{1,0:T(8,128)S(1)} %reshape.239, bf16[24,6,1024]{2,0,1:T(8,128)(2,1)} %all_to_all.19, bf16[24,2048]{1,0:T(8,128)(2,1)S(1)} %copy-done.3), kind=kOutput, calls=%fused_computation.49 | convolution fusion | flops 101105640 | bytes 4636768 | tf_op jit(solution)/shard_map/dot_general | solution.py:177
  149.1 0.7 multiply_convert_fusion
  149.8 0.7 compare_reduce_fusion
  150.7 0.2 reduce_window_sum.23
  150.9 0.8 constant_dynamic-slice_fusion.1
  151.8 0.8 constant_dynamic-slice_fusion
  152.5 0.7 select_reduce_fusion
  153.2 9.3 %broadcast_multiply_fusion = (f32[24,16,64,64]{3,2,1,0:T(8,128)}, f32[24,16,64,64]{3,2,1,0:T(8,128)}) fusion(f32[24,16,64]{2,1,0:T(8,128)S(1)} %get-tuple-element.4, f32[24,16,64]{2,1,0:T(8,128)S(1)} %reshape.246, f32[24,16,64]{2,1,0:T(8,128)S(1)} %get-tuple-element.2, f32[24,16,64]{2,1,0:T(8,128)S(1)} %bitcast.96), kind=kLoop, calls=%fused_computation.6 | loop fusion | flops 3145728 | bytes 12976128 | tf_op jit(solution)/shard_map/mul | solution.py:57
  162.5 10.8 %mul.247 = f32[24,16,4096]{2,1,0:T(8,128)} reshape(f32[24,16,64,64]{3,2,1,0:T(8,128)} %get-tuple-element.14) | data formatting | bytes 12582912 | tf_op jit(solution)/shard_map/mul | solution.py:57
  173.3 10.9 %mul.246 = f32[24,16,4096]{2,1,0:T(8,128)} reshape(f32[24,16,64,64]{3,2,1,0:T(8,128)} %get-tuple-element.15) | data formatting | bytes 12582912 | tf_op jit(solution)/shard_map/mul | solution.py:56
  184.3 5.4 %mul.206 = f32[24,16,64,64]{3,2,1,0:T(8,128)} broadcast(f32[24,16,64]{2,1,0:T(8,128)S(1)} %copy-done.5), dimensions={0,1,3} | broadcast | bytes 6389760 | tf_op jit(solution)/shard_map/mul | solution.py:55
  189.6 10.9 %mul.244 = f32[24,16,4096]{2,1,0:T(8,128)} reshape(f32[24,16,64,64]{3,2,1,0:T(8,128)} %mul.206) | data formatting | bytes 12582912 | tf_op jit(solution)/shard_map/mul | solution.py:55
  200.6 9.7 %all-gather.5.cloned.1.call-done = bf16[768,2048]{1,0:T(8,128)(2,1)} async-done(((bf16[24,2048]{1,0:T(8,128)(2,1)}), bf16[768,2048]{1,0:T(8,128)(2,1)}) %all-gather.5.cloned.1.call-update) | async-done | bytes 3145744 | tf_op jit(solution)/shard_map/all_gather | solution.py:188
  210.3 2.7 %convolution_convert_fusion.1 = bf16[32,4,2048]{2,1,0:T(4,128)(2,1)S(1)} fusion(bf16[32,24,2048]{2,1,0:T(8,128)(2,1)} %bitcast.91, s32[32,24]{1,0:T(8,128)S(1)} %sub.39, pred[32,24]{1,0:T(8,128)(4,1)S(1)} %broadcast_compare_fusion), kind=kOutput, calls=%fused_computation.10 | convolution fusion | flops 12857344 | bytes 3673856 | tf_op jit(solution)/shard_map/snc,snd->scd/dot_general | solution.py:107
  213.1 2.7 %fusion.15 = f32[128,512]{1,0:T(8,128)} fusion(bf16[128,2048]{1,0:T(8,128)(2,1)S(1)} %reshape.241, bf16[1,2048,512]{2,1,0:T(8,128)(2,1)} %param.40), kind=kOutput, calls=%fused_computation.23 | convolution fusion | flops 268435456 | bytes 2883584 | tf_op jit(solution)/shard_map/dot_general | solution.py:17
  215.8 2.4 convolution_convert_fusion
  218.3 1.0 reshape.242
  219.2 3.3 %all-to-all-start.1 = ((bf16[32,4,2048]{2,1,0:T(4,128)(2,1)}), bf16[32,4,2048]{2,1,0:T(4,128)(2,1)S(1)}, u32[]{:S(2)}, u32[]{:S(2)}) async-start(bf16[32,4,2048]{2,1,0:T(4,128)(2,1)} %reshape.242), calls=%async_computation.1 | async-start | bytes 1048576 | tf_op jit(solution)/shard_map/all_to_all | solution.py:200
  222.6 14.2 %subtract_add_fusion = f32[24,16,4096]{2,1,0:T(8,128)} fusion(f32[24,16,4096]{2,1,0:T(8,128)} %mul.247, f32[24,16,4096]{2,1,0:T(8,128)} %mul.246, f32[24,16,4096]{2,1,0:T(8,128)} %param.35, f32[24,16,4096]{2,1,0:T(8,128)} %mul.244), kind=kLoop, calls=%fused_computation.5 | loop fusion | flops 4718592 | bytes 31457280 | tf_op jit(solution)/shard_map/add | solution.py:55
  236.8 2.0 fusion.74
  238.8 3.0 %fusion.9 = f32[24,2048]{1,0:T(8,128)S(1)} fusion(f32[24,2048]{1,0:T(8,128)S(1)} %get-tuple-element.13, bf16[512,2048]{1,0:T(8,128)(2,1)} %param.45, bf16[24,2048]{1,0:T(8,128)(2,1)S(1)} %copy-done.2, bf16[2048,512]{1,0:T(8,128)(2,1)} %param.44, f32[24,512]{1,0:T(8,128)S(1)} %fusion.74), kind=kOutput, calls=%fused_computation.16 | convolution fusion | flops 100884480 | bytes 4734976 | tf_op jit(solution)/shard_map/dot_general | solution.py:20
  241.8 1.3 fusion.7
  (60 shorter events, 1.8 us)
Async XLA Ops:
  7.2 208.7 %copy-start = (bf16[1,512,2048]{2,1,0:T(8,128)(2,1)S(1)}, bf16[1,512,2048]{2,1,0:T(8,128)(2,1)}, u32[]{:S(2)}) copy-start(bf16[1,512,2048]{2,1,0:T(8,128)(2,1)} %param.42) | copy-start | bytes 6291460
  7.2 66.1 %all-gather.3.cloned.1.call-start = ((), (), s32[]{:S(2)}) async-start(), calls=%async_computation.2 | async-start | bytes 3244032 | tf_op jit(solution)/shard_map/all_gather | solution.py:159
  81.6 14.8 %all-to-all-start = ((bf16[32,2,2304]{2,1,0:T(2,128)(2,1)}), bf16[32,2,2304]{2,1,0:T(2,128)(2,1)S(1)}, u32[]{:S(2)}, u32[]{:S(2)}) async-start(bf16[32,2,2304]{2,1,0:T(2,128)(2,1)} %reshape.259), calls=%async_computation | async-start | bytes 589824 | tf_op jit(solution)/shard_map/all_to_all | solution.py:163
  85.0 11.1 %copy-start.8 = (f32[1024]{0:T(1024)S(1)}, f32[1024]{0:T(1024)}, u32[]{:S(2)}) copy-start(f32[1024]{0:T(1024)} %param.31) | copy-start | bytes 12292
  85.0 11.2 %copy-start.9 = (f32[1024]{0:T(1024)S(1)}, f32[1024]{0:T(1024)}, u32[]{:S(2)}) copy-start(f32[1024]{0:T(1024)} %param.32) | copy-start | bytes 12292
  85.0 11.3 %copy-start.10 = (f32[1024]{0:T(1024)S(1)}, f32[1024]{0:T(1024)}, u32[]{:S(2)}) copy-start(f32[1024]{0:T(1024)} %param.33) | copy-start | bytes 12292
  85.0 11.3 %copy-start.11 = (f32[1024]{0:T(1024)S(1)}, f32[1024]{0:T(1024)}, u32[]{:S(2)}) copy-start(f32[1024]{0:T(1024)} %param.34) | copy-start | bytes 12292
  85.0 11.4 %copy-start.12 = (bf16[2048]{0:T(1024)(128)(2,1)S(1)}, bf16[2048]{0:T(1024)(128)(2,1)}, u32[]{:S(2)}) copy-start(bf16[2048]{0:T(1024)(128)(2,1)} %param.37) | copy-start | bytes 12292
  85.0 125.3 %all-gather.5.cloned.1.call-start = ((), (), s32[]{:S(2)}) async-start(), calls=%async_computation.3 | async-start | bytes 3244032 | tf_op jit(solution)/shard_map/all_gather | solution.py:188
  105.3 22.9 %copy-start.4 = (f32[24,16,64]{2,1,0:T(8,128)}, f32[24,16,64]{2,1,0:T(8,128)S(1)}, u32[]{:S(2)}) copy-start(f32[24,16,64]{2,1,0:T(8,128)S(1)} %fusion.41) | copy-start | bytes 294916
  105.5 22.8 %copy-start.1 = (f32[24,16,64,64]{3,2,1,0:T(8,128)S(1)}, f32[24,16,64,64]{3,2,1,0:T(8,128)}, u32[]{:S(2)}) copy-start(f32[24,16,64,64]{3,2,1,0:T(8,128)} %reshape.237) | copy-start | bytes 18874372
  105.5 22.8 %copy-start.6 = (bf16[24,16,64,1]{2,3,1,0:T(2,128)(2,1)S(1)}, bf16[24,16,64,1]{2,3,1,0:T(2,128)(2,1)}, u32[]{:S(2)}) copy-start(bf16[24,16,64,1]{2,3,1,0:T(2,128)(2,1)} %reshape.258) | copy-start | bytes 147460
  128.3 17.8 %copy-start.3 = (bf16[24,2048]{1,0:T(8,128)(2,1)S(1)}, bf16[24,2048]{1,0:T(8,128)(2,1)}, u32[]{:S(2)}) copy-start(bf16[24,2048]{1,0:T(8,128)(2,1)} %param.23) | copy-start | bytes 294916
  173.3 10.9 %copy-start.5 = (f32[24,16,64]{2,1,0:T(8,128)S(1)}, f32[24,16,64]{2,1,0:T(8,128)}, u32[]{:S(2)}) copy-start(f32[24,16,64]{2,1,0:T(8,128)} %copy-done.4) | copy-start | bytes 294916
  219.2 22.5 %all-to-all-start.1 = ((bf16[32,4,2048]{2,1,0:T(4,128)(2,1)}), bf16[32,4,2048]{2,1,0:T(4,128)(2,1)S(1)}, u32[]{:S(2)}, u32[]{:S(2)}) async-start(bf16[32,4,2048]{2,1,0:T(4,128)(2,1)} %reshape.242), calls=%async_computation.1 | async-start | bytes 1048576 | tf_op jit(solution)/shard_map/all_to_all | solution.py:200
  222.6 14.2 %copy-start.2 = (bf16[24,2048]{1,0:T(8,128)(2,1)S(1)}, bf16[24,2048]{1,0:T(8,128)(2,1)}, u32[]{:S(2)}) copy-start(bf16[24,2048]{1,0:T(8,128)(2,1)} %multiply_convert_fusion) | copy-start | bytes 294916
  236.8 5.0 %copy-start.7 = (f32[24,32]{1,0:T(8,128)S(1)}, f32[24,32]{1,0:T(8,128)}, u32[]{:S(2)}) copy-start(f32[24,32]{1,0:T(8,128)} %select_reduce_fusion) | copy-start | bytes 9220
Sparse Core Ops, SparseCore 0:
  11.4 61.7 all-gather.2
  150.0 60.2 all-gather.4
where the time goes:
time: 251 us; the launch traced here: 250 us
  local copies, waits for them, and re-layouts  70.5 us (28%)
  waiting for transfers between devices  66.8 us (27%)
  matrix products  59.4 us (24%)
  other arithmetic  32 us (13%)
  between operations  14.4 us (6%)
  starting transfers between devices  6.93 us (3%)
    all_gather x1, waiting for transfers between devices, per_device(): lax.all_gather(normed, 'ep', axis=0, tiled=True)  57 us
    dot_general x1, matrix products, attention_mixer(): jnp.einsum('nhvk,nhk->nhv', matrix, unit_key, precision=lax.Precision.HIG...  22.8 us
    dot_general x1, matrix products, attention_mixer(): jnp.einsum('nhvk,nhk->nhv', matrix, receptance_head, precision=lax.Precis...  16.5 us
    mul x2, local copies, waits for them, and re-layouts, attention_mixer(): matrix * heads(decay)[:, :, None, :]  16.3 us
    add x1, other arithmetic, attention_mixer(): matrix * heads(decay)[:, :, None, :]  14.2 us
    mul x1, local copies, waits for them, and re-layouts, attention_mixer(): recalled[..., None] * removal[:, :, None, :]  10.9 us
    reshape x1, local copies, waits for them, and re-layouts, attention_mixer(): matrix = head_state.reshape(tally_value, HEAD_COUNT, HEAD_SIZE, HEAD_SIZE)  10.8 us
    mul x1, local copies, waits for them, and re-layouts, attention_mixer(): head_value[..., None] * rate_scaled_key[:, :, None, :]  10.8 us
  transfers between devices with their start and end apart: 4, of which 2 were waited for; matrix products, arithmetic and copies ran while one was open for 35% of the time, Pallas kernels for 0%

commit v1 on v0

--- a/solution.py
+++ b/solution.py
@@ -156,7 +156,9 @@
     )
     local_cols = jnp.einsum(
         "td,drc->trc",
-        lax.all_gather(normed, "ep", axis=0, tiled=True),
+        jnp.concatenate(
+            lax.all_to_all(jnp.stack([normed] * lax.axis_size("ep")), "ep", 0, 0), axis=0
+        ),
         stacked,
         preferred_element_type=jnp.float32,
     ).astype(jnp.bfloat16)

time: 251 us -> 270 us (1.076)
  waiting for transfers between devices: 66.8 us -> 77.1 us
  starting transfers between devices: 6.93 us -> 15 us
    all_to_all x0 -> x1, waiting for transfers between devices: none -> 67.3 us  [per_device(): lax.all_to_all(jnp.stack([normed] * lax.axis_size('ep')), 'ep', 0, 0)]
    all_gather x1 -> x0, waiting for transfers between devices: 57 us -> none  [per_device(): lax.all_gather(normed, 'ep', axis=0, tiled=True)]
    all_to_all x0 -> x1, starting transfers between devices: none -> 7.45 us  [per_device(): lax.all_to_all(jnp.stack([normed] * lax.axis_size('ep')), 'ep', 0, 0)]
    unnamed x33 -> x45, local copies, waits for them, and re-layouts: 10.3 us -> 9.05 us
  transfers between devices with their start and end apart: 4 -> 4, of which waited for: 2 -> 2; matrix products, arithmetic and copies ran while one was open for 35% -> 32% of each run, Pallas kernels for 0% -> 0%
where the time goes in v1:
time: 270 us; the launch traced here: 269 us
  waiting for transfers between devices  77.1 us (29%)
  local copies, waits for them, and re-layouts  71 us (26%)
  matrix products  59.6 us (22%)
  other arithmetic  31.3 us (12%)
  starting transfers between devices  15 us (6%)
  between operations  14.4 us (5%)
    all_to_all x1, waiting for transfers between devices, per_device(): lax.all_to_all(jnp.stack([normed] * lax.axis_size('ep')), 'ep', 0, 0)  67.3 us
    dot_general x1, matrix products, attention_mixer(): jnp.einsum('nhvk,nhk->nhv', matrix, unit_key, precision=lax.Precision.HIG...  22.8 us
    dot_general x1, matrix products, attention_mixer(): jnp.einsum('nhvk,nhk->nhv', matrix, receptance_head, precision=lax.Precis...  16.5 us
    mul x2, local copies, waits for them, and re-layouts, attention_mixer(): matrix * heads(decay)[:, :, None, :]  16.3 us
    add x1, other arithmetic, attention_mixer(): matrix * heads(decay)[:, :, None, :]  14.2 us
    mul x1, local copies, waits for them, and re-layouts, attention_mixer(): recalled[..., None] * removal[:, :, None, :]  10.9 us
    reshape x1, local copies, waits for them, and re-layouts, attention_mixer(): matrix = head_state.reshape(tally_value, HEAD_COUNT, HEAD_SIZE, HEAD_SIZE)  10.9 us
    mul x1, local copies, waits for them, and re-layouts, attention_mixer(): head_value[..., None] * rate_scaled_key[:, :, None, :]  10.8 us
  transfers between devices with their start and end apart: 4, of which 2 were waited for; matrix products, arithmetic and copies ran while one was open for 32% of the time, Pallas kernels for 0%

profile of v1, /device:TPU:0, one launch (start us, length us, event | category | flops | bytes accessed | tf_op | source)
XLA Modules:
  0.0 268.5 jit_solution(2481296854341186128)
XLA Ops:
  7.2 0.8 convert_element_type.171
  8.0 1.0 fusion.34
  9.0 1.0 fusion.36
  10.1 2.1 stack.16
  12.1 7.4 %all-to-all-start = ((bf16[32,24,2048]{2,1,0:T(8,128)(2,1)}), bf16[32,24,2048]{2,1,0:T(8,128)(2,1)}, u32[]{:S(2)}, u32[]{:S(2)}) async-start(bf16[32,24,2048]{2,1,0:T(8,128)(2,1)} %stack.16), calls=%async_computation | async-start | bytes 6291456 | tf_op jit(solution)/shard_map/all_to_all | solution.py:160
  19.6 0.7 bitcast_dynamic-update-slice_fusion.5
  20.3 0.7 bitcast_dynamic-update-slice_fusion.4
  20.9 0.7 bitcast_dynamic-update-slice_fusion.3
  21.6 0.7 bitcast_dynamic-update-slice_fusion.2
  22.3 0.7 bitcast_dynamic-update-slice_fusion.1
  22.9 0.7 bitcast_dynamic-update-slice_fusion
  23.6 67.3 %all-to-all-done = bf16[32,24,2048]{2,1,0:T(8,128)(2,1)} async-done(((bf16[32,24,2048]{2,1,0:T(8,128)(2,1)}), bf16[32,24,2048]{2,1,0:T(8,128)(2,1)}, u32[]{:S(2)}, u32[]{:S(2)}) %all-to-all-start) | async-done | bytes 3145760 | tf_op jit(solution)/shard_map/all_to_all | solution.py:160
  90.9 3.3 %fusion.72 = f32[768,192]{0,1:S(1)} fusion(bf16[768,2048]{1,0:T(8,128)(2,1)} %bitcast, bf16[2048,192]{0,1:T(8,128)(2,1)} %bitcast.7), kind=kOutput, calls=%fused_computation.110 | convolution fusion | flops 603979776 | bytes 4521984
  94.2 1.8 copy.38
  96.0 3.4 %reshape.265 = bf16[32,2,2304]{2,1,0:T(2,128)(2,1)} reshape(bf16[768,6,32]{2,1,0:T(8,128)(2,1)} %copy.38) | data formatting | bytes 589824
  99.5 4.0 %all-to-all-start.1 = ((bf16[32,2,2304]{2,1,0:T(2,128)(2,1)}), bf16[32,2,2304]{2,1,0:T(2,128)(2,1)S(1)}, u32[]{:S(2)}, u32[]{:S(2)}) async-start(bf16[32,2,2304]{2,1,0:T(2,128)(2,1)} %reshape.265), calls=%async_computation.1 | async-start | bytes 589824 | tf_op jit(solution)/shard_map/all_to_all | solution.py:165
  103.6 0.2 all-gather.2.cloned.1.call-start
  103.8 10.9 %reshape.242 = f32[24,16,64,64]{3,2,1,0:T(8,128)} reshape(f32[24,16,4096]{2,1,0:T(8,128)} %param.35) | data formatting | bytes 12582912 | tf_op jit(solution)/shard_map/reshape | solution.py:52
  115.0 2.2 reshape.266
  117.2 2.2 copy.40
  119.3 1.9 all_to_all.23
  121.3 0.9 slice_convert_fusion.2
  122.2 0.8 reshape.264
  124.0 22.8 %fusion.73 = f32[24,16,1,64]{3,2,1,0:T(1,128)S(1)} fusion(f32[24,16,64,1]{2,3,1,0:T(1,128)S(1)} %bitcast.98, f32[24,16,64,64]{3,2,1,0:T(8,128)} %reshape.242), kind=kOutput, calls=%fused_computation.111 | convolution fusion | flops 18874368 | bytes 6488064 | tf_op jit(solution)/shard_map/nhvk,nhk->nhv/dot_general | solution.py:53
  146.9 16.5 %fusion.1 = f32[24,16,1,64]{3,2,1,0:T(1,128)S(1)} fusion(bf16[24,16,64,1]{2,3,1,0:T(2,128)(2,1)S(1)} %copy-done.6, f32[24,16,64,64]{3,2,1,0:T(8,128)S(1)} %copy-done.1, f32[24,16,64]{2,1,0:T(8,128)S(1)} %fusion.41, f32[24,16,64]{2,1,0:T(8,128)S(1)} %get-tuple-element.2, f32[24,16,64]{2,1,0:T(8,128)S(1)} %bitcast.96, f32[24,16,64]{2,1,0:T(8,128)S(1)} %get-tuple-element.4, ...), kind=kOutput, calls=%fused_computation.1 | convolution fusion | flops 26738688 | bytes 6930432 | tf_op jit(solution)/shard_map/nhvk,nhk->nhv/dot_general | solution.py:59
  163.5 0.2 multiply_reduce_fusion.1
  163.8 0.8 fusion.24
  164.7 3.0 %multiply_reduce_fusion = (f32[24]{0:T(128)S(1)}, f32[24,2048]{1,0:T(8,128)S(1)}) fusion(bf16[1024,2048]{1,0:T(8,128)(2,1)} %param.36, f32[24,1024]{1,0:T(8,128)S(1)} %reshape.245, bf16[24,6,1024]{2,0,1:T(8,128)(2,1)} %all_to_all.23, bf16[24,2048]{1,0:T(8,128)(2,1)S(1)} %copy-done.3), kind=kOutput, calls=%fused_computation.49 | convolution fusion | flops 101105640 | bytes 4636768 | tf_op jit(solution)/shard_map/dot_general | solution.py:179
  167.7 0.7 multiply_convert_fusion
  168.4 0.7 compare_reduce_fusion
  169.5 0.8 constant_dynamic-slice_fusion.1
  170.4 0.8 constant_dynamic-slice_fusion
  171.1 0.7 select_reduce_fusion
  171.8 9.3 %broadcast_multiply_fusion = (f32[24,16,64,64]{3,2,1,0:T(8,128)}, f32[24,16,64,64]{3,2,1,0:T(8,128)}) fusion(f32[24,16,64]{2,1,0:T(8,128)S(1)} %get-tuple-element.4, f32[24,16,64]{2,1,0:T(8,128)S(1)} %reshape.252, f32[24,16,64]{2,1,0:T(8,128)S(1)} %get-tuple-element.2, f32[24,16,64]{2,1,0:T(8,128)S(1)} %bitcast.97), kind=kLoop, calls=%fused_computation.6 | loop fusion | flops 3145728 | bytes 12976128 | tf_op jit(solution)/shard_map/mul | solution.py:57
  181.1 10.8 %mul.247 = f32[24,16,4096]{2,1,0:T(8,128)} reshape(f32[24,16,64,64]{3,2,1,0:T(8,128)} %get-tuple-element.14) | data formatting | bytes 12582912 | tf_op jit(solution)/shard_map/mul | solution.py:57
  191.9 10.9 %mul.246 = f32[24,16,4096]{2,1,0:T(8,128)} reshape(f32[24,16,64,64]{3,2,1,0:T(8,128)} %get-tuple-element.15) | data formatting | bytes 12582912 | tf_op jit(solution)/shard_map/mul | solution.py:56
  202.8 5.4 %mul.206 = f32[24,16,64,64]{3,2,1,0:T(8,128)} broadcast(f32[24,16,64]{2,1,0:T(8,128)S(1)} %copy-done.5), dimensions={0,1,3} | broadcast | bytes 6389760 | tf_op jit(solution)/shard_map/mul | solution.py:55
  208.2 10.9 %mul.244 = f32[24,16,4096]{2,1,0:T(8,128)} reshape(f32[24,16,64,64]{3,2,1,0:T(8,128)} %mul.206) | data formatting | bytes 12582912 | tf_op jit(solution)/shard_map/mul | solution.py:55
  219.1 9.8 %all-gather.2.cloned.1.call-done = bf16[768,2048]{1,0:T(8,128)(2,1)} async-done(((bf16[24,2048]{1,0:T(8,128)(2,1)}), bf16[768,2048]{1,0:T(8,128)(2,1)}) %all-gather.2.cloned.1.call-update) | async-done | bytes 3145744 | tf_op jit(solution)/shard_map/all_gather | solution.py:190
  228.9 2.7 convolution_convert_fusion.1
  231.7 2.7 %fusion.15 = f32[128,512]{1,0:T(8,128)} fusion(bf16[128,2048]{1,0:T(8,128)(2,1)S(1)} %reshape.247, bf16[1,2048,512]{2,1,0:T(8,128)(2,1)} %param.40), kind=kOutput, calls=%fused_computation.23 | convolution fusion | flops 268435456 | bytes 2883584 | tf_op jit(solution)/shard_map/dot_general | solution.py:17
  234.4 2.4 convolution_convert_fusion
  236.9 1.0 reshape.248
  237.8 3.3 %all-to-all-start.2 = ((bf16[32,4,2048]{2,1,0:T(4,128)(2,1)}), bf16[32,4,2048]{2,1,0:T(4,128)(2,1)S(1)}, u32[]{:S(2)}, u32[]{:S(2)}) async-start(bf16[32,4,2048]{2,1,0:T(4,128)(2,1)} %reshape.248), calls=%async_computation.2 | async-start | bytes 1048576 | tf_op jit(solution)/shard_map/all_to_all | solution.py:202
  241.2 14.2 %subtract_add_fusion = f32[24,16,4096]{2,1,0:T(8,128)} fusion(f32[24,16,4096]{2,1,0:T(8,128)} %mul.247, f32[24,16,4096]{2,1,0:T(8,128)} %mul.246, f32[24,16,4096]{2,1,0:T(8,128)} %param.35, f32[24,16,4096]{2,1,0:T(8,128)} %mul.244), kind=kLoop, calls=%fused_computation.5 | loop fusion | flops 4718592 | bytes 31457280 | tf_op jit(solution)/shard_map/add | solution.py:55
  255.4 2.0 fusion.74
  257.4 3.0 %fusion.9 = f32[24,2048]{1,0:T(8,128)S(1)} fusion(f32[24,2048]{1,0:T(8,128)S(1)} %get-tuple-element.13, bf16[512,2048]{1,0:T(8,128)(2,1)} %param.45, bf16[24,2048]{1,0:T(8,128)(2,1)S(1)} %copy-done.2, bf16[2048,512]{1,0:T(8,128)(2,1)} %param.44, f32[24,512]{1,0:T(8,128)S(1)} %fusion.74), kind=kOutput, calls=%fused_computation.16 | convolution fusion | flops 100884480 | bytes 4734976 | tf_op jit(solution)/shard_map/dot_general | solution.py:20
  260.4 1.3 fusion.7
  (72 shorter events, 2.2 us)
Async XLA Ops:
  7.2 227.3 %copy-start = (bf16[1,512,2048]{2,1,0:T(8,128)(2,1)S(1)}, bf16[1,512,2048]{2,1,0:T(8,128)(2,1)}, u32[]{:S(2)}) copy-start(bf16[1,512,2048]{2,1,0:T(8,128)(2,1)} %param.42) | copy-start | bytes 6291460
  10.0 9.5 %copy-start.7 = (bf16[2048,32]{0,1:T(8,128)(2,1)S(1)}, bf16[2048,32]{0,1:T(8,128)(2,1)}, u32[]{:S(2)}) copy-start(bf16[2048,32]{0,1:T(8,128)(2,1)} %param.25) | copy-start | bytes 393220
  10.1 10.2 %copy-start.8 = (bf16[2048,32]{0,1:T(8,128)(2,1)S(1)}, bf16[2048,32]{0,1:T(8,128)(2,1)}, u32[]{:S(2)}) copy-start(bf16[2048,32]{0,1:T(8,128)(2,1)} %param.26) | copy-start | bytes 393220
  12.1 8.8 %copy-start.9 = (bf16[2048,32]{0,1:T(8,128)(2,1)S(1)}, bf16[2048,32]{0,1:T(8,128)(2,1)}, u32[]{:S(2)}) copy-start(bf16[2048,32]{0,1:T(8,128)(2,1)} %param.27) | copy-start | bytes 393220
  12.1 9.5 %copy-start.10 = (bf16[2048,32]{0,1:T(8,128)(2,1)S(1)}, bf16[2048,32]{0,1:T(8,128)(2,1)}, u32[]{:S(2)}) copy-start(bf16[2048,32]{0,1:T(8,128)(2,1)} %param.28) | copy-start | bytes 393220
  12.1 10.1 %copy-start.11 = (bf16[2048,32]{0,1:T(8,128)(2,1)S(1)}, bf16[2048,32]{0,1:T(8,128)(2,1)}, u32[]{:S(2)}) copy-start(bf16[2048,32]{0,1:T(8,128)(2,1)} %param.29) | copy-start | bytes 393220
  12.1 10.8 %copy-start.12 = (bf16[2048,32]{0,1:T(8,128)(2,1)S(1)}, bf16[2048,32]{0,1:T(8,128)(2,1)}, u32[]{:S(2)}) copy-start(bf16[2048,32]{0,1:T(8,128)(2,1)} %param.30) | copy-start | bytes 393220
  12.1 78.8 %all-to-all-start = ((bf16[32,24,2048]{2,1,0:T(8,128)(2,1)}), bf16[32,24,2048]{2,1,0:T(8,128)(2,1)}, u32[]{:S(2)}, u32[]{:S(2)}) async-start(bf16[32,24,2048]{2,1,0:T(8,128)(2,1)} %stack.16), calls=%async_computation | async-start | bytes 6291456 | tf_op jit(solution)/shard_map/all_to_all | solution.py:160
  99.5 15.5 %all-to-all-start.1 = ((bf16[32,2,2304]{2,1,0:T(2,128)(2,1)}), bf16[32,2,2304]{2,1,0:T(2,128)(2,1)S(1)}, u32[]{:S(2)}, u32[]{:S(2)}) async-start(bf16[32,2,2304]{2,1,0:T(2,128)(2,1)} %reshape.265), calls=%async_computation.1 | async-start | bytes 589824 | tf_op jit(solution)/shard_map/all_to_all | solution.py:165
  103.5 11.1 %copy-start.14 = (f32[1024]{0:T(1024)S(1)}, f32[1024]{0:T(1024)}, u32[]{:S(2)}) copy-start(f32[1024]{0:T(1024)} %param.31) | copy-start | bytes 12292
  103.5 11.2 %copy-start.15 = (f32[1024]{0:T(1024)S(1)}, f32[1024]{0:T(1024)}, u32[]{:S(2)}) copy-start(f32[1024]{0:T(1024)} %param.32) | copy-start | bytes 12292
  103.6 11.3 %copy-start.16 = (f32[1024]{0:T(1024)S(1)}, f32[1024]{0:T(1024)}, u32[]{:S(2)}) copy-start(f32[1024]{0:T(1024)} %param.33) | copy-start | bytes 12292
  103.6 11.3 %copy-start.17 = (f32[1024]{0:T(1024)S(1)}, f32[1024]{0:T(1024)}, u32[]{:S(2)}) copy-start(f32[1024]{0:T(1024)} %param.34) | copy-start | bytes 12292
  103.6 11.4 %copy-start.18 = (bf16[2048]{0:T(1024)(128)(2,1)S(1)}, bf16[2048]{0:T(1024)(128)(2,1)}, u32[]{:S(2)}) copy-start(bf16[2048]{0:T(1024)(128)(2,1)} %param.37) | copy-start | bytes 12292
  103.6 125.3 %all-gather.2.cloned.1.call-start = ((), (), s32[]{:S(2)}) async-start(), calls=%async_computation.3 | async-start | bytes 3244032 | tf_op jit(solution)/shard_map/all_gather | solution.py:190
  123.9 23.0 %copy-start.4 = (f32[24,16,64]{2,1,0:T(8,128)}, f32[24,16,64]{2,1,0:T(8,128)S(1)}, u32[]{:S(2)}) copy-start(f32[24,16,64]{2,1,0:T(8,128)S(1)} %fusion.41) | copy-start | bytes 294916
  124.0 22.8 %copy-start.1 = (f32[24,16,64,64]{3,2,1,0:T(8,128)S(1)}, f32[24,16,64,64]{3,2,1,0:T(8,128)}, u32[]{:S(2)}) copy-start(f32[24,16,64,64]{3,2,1,0:T(8,128)} %reshape.242) | copy-start | bytes 18874372
  124.0 22.8 %copy-start.6 = (bf16[24,16,64,1]{2,3,1,0:T(2,128)(2,1)S(1)}, bf16[24,16,64,1]{2,3,1,0:T(2,128)(2,1)}, u32[]{:S(2)}) copy-start(bf16[24,16,64,1]{2,3,1,0:T(2,128)(2,1)} %reshape.264) | copy-start | bytes 147460
  146.9 17.8 %copy-start.3 = (bf16[24,2048]{1,0:T(8,128)(2,1)S(1)}, bf16[24,2048]{1,0:T(8,128)(2,1)}, u32[]{:S(2)}) copy-start(bf16[24,2048]{1,0:T(8,128)(2,1)} %param.23) | copy-start | bytes 294916
  191.9 10.9 %copy-start.5 = (f32[24,16,64]{2,1,0:T(8,128)S(1)}, f32[24,16,64]{2,1,0:T(8,128)}, u32[]{:S(2)}) copy-start(f32[24,16,64]{2,1,0:T(8,128)} %copy-done.4) | copy-start | bytes 294916
  237.8 22.5 %all-to-all-start.2 = ((bf16[32,4,2048]{2,1,0:T(4,128)(2,1)}), bf16[32,4,2048]{2,1,0:T(4,128)(2,1)S(1)}, u32[]{:S(2)}, u32[]{:S(2)}) async-start(bf16[32,4,2048]{2,1,0:T(4,128)(2,1)} %reshape.248), calls=%async_computation.2 | async-start | bytes 1048576 | tf_op jit(solution)/shard_map/all_to_all | solution.py:202
  241.2 14.2 %copy-start.2 = (bf16[24,2048]{1,0:T(8,128)(2,1)S(1)}, bf16[24,2048]{1,0:T(8,128)(2,1)}, u32[]{:S(2)}) copy-start(bf16[24,2048]{1,0:T(8,128)(2,1)} %multiply_convert_fusion) | copy-start | bytes 294916
  255.4 5.0 %copy-start.13 = (f32[24,32]{1,0:T(8,128)S(1)}, f32[24,32]{1,0:T(8,128)}, u32[]{:S(2)}) copy-start(f32[24,32]{1,0:T(8,128)} %select_reduce_fusion) | copy-start | bytes 9220
Sparse Core Ops, SparseCore 0:
  168.6 60.2 all-gather.1
